TPU v7x, 32 devices: a whole 2x2x4 slice. The times are simulated.
32 devices in a mesh: fs: 8 (over z, core), tp: 4 (over y, x).
Axes of the slice: x: 2, y: 2, z: 4, core: 2. Of those that a mesh axis runs over, the one named last changes fastest.
Arguments:
- attn_out: bfloat16 [12288, 2048], P('fs', 'tp'), may hold values from -6 to 6
- out_cot: bfloat16 [12288, 4096], P('fs', 'tp'), may hold values from -6 to 6
- latent: bfloat16 [12288, 1024], P('fs', 'tp'), may hold values from -6 to 6
- value_cot: bfloat16 [12288, 2048], P('fs', 'tp'), may hold values from -6 to 6
- out_weight: float32 [2048, 4096], P('fs', 'tp'), may hold values from -0.125 to 0.125
- value_up_matrix: float32 [1024, 2048], P('fs', 'tp'), may hold values from -0.1875 to 0.1875
- out_basis: bfloat16 [2048, 256], P('fs'), as said below
- value_basis: bfloat16 [1024, 256], P('fs'), as said below
- out_mean: float32 [256, 4096], P(None, 'tp'), may hold values from -2660.43 to 2660.43
- out_square: float32 [256, 4096], P(None, 'tp'), may hold values from 12288 to 2457600, as said below
- value_mean: float32 [256, 2048], P(None, 'tp'), may hold values from -2660.43 to 2660.43
- value_square: float32 [256, 2048], P(None, 'tp'), may hold values from 12288 to 2457600, as said below
Outputs:
- out_step: float32 [2048, 4096], P('fs', 'tp')
- out_new: float32 [2048, 4096], P('fs', 'tp')
- out_copy: bfloat16 [2048, 4096], P(None, 'tp')
- out_mean_new: float32 [256, 4096], P(None, 'tp')
- out_square_new: float32 [256, 4096], P(None, 'tp')
- value_step: float32 [1024, 2048], P('fs', 'tp')
- value_new: float32 [1024, 2048], P('fs', 'tp')
- value_copy: bfloat16 [1024, 2048], P(None, 'tp')
- value_mean_new: float32 [256, 2048], P(None, 'tp')
- value_square_new: float32 [256, 2048], P(None, 'tp')
Inputs may be any that keep to these rules, and one draw needn't show every extreme that they name: `out_basis`: factors of full rank, rows of differing scales. `value_basis`: factors of full rank, rows of differing scales. `out_square`: Positive. `value_square`: Positive.
All inputs are finite; a program needn't handle non-finite values.
Results may differ from a plain program's by a relative error of at most 0.012.
Values may be sent and summed in bfloat16 or wider, within the bound.
A program may use at most 64 MiB of HBM per device.

v0:
```python
import jax
import jax.numpy as jnp
from jax import lax
from jax.sharding import PartitionSpec as P

LEARN_RATE = 0.01
MEAN_DECAY = 0.8
BETA_SQUARE = 0.9
EPS_RMS = 1e-06


def moments(proj, mean_in, square_in):
    mean_new = MEAN_DECAY * mean_in + (1.0 - MEAN_DECAY) * proj
    square_new = BETA_SQUARE * square_in + (1.0 - BETA_SQUARE) * proj * proj
    return (mean_new, square_new, mean_new / jnp.sqrt(square_new))


def split_product(lifted, cotangent):
    upper = lifted.astype(jnp.bfloat16)
    lower = (lifted - upper.astype(jnp.float32)).astype(jnp.bfloat16)
    first = jnp.dot(upper.T, cotangent, preferred_element_type=jnp.float32)
    return first + jnp.dot(lower.T, cotangent, preferred_element_type=jnp.float32)


def per_device(
    attn_out,
    out_cot,
    latent,
    value_cot,
    out_weight,
    value_up_matrix,
    out_basis,
    value_basis,
    out_mean,
    out_square,
    value_mean,
    value_square,
):
    width_out = out_cot.shape[1]
    head_cols = value_cot.shape[1]
    rows_out = out_basis.shape[0]
    rows_value = value_basis.shape[0]
    all_heads, all_latent = (
        lax.all_gather(attn_out, "tp", axis=1, tiled=True),
        lax.all_gather(latent, "tp", axis=1, tiled=True),
    )
    whole_o, whole_v = (
        lax.all_gather(out_basis, "fs", axis=0, tiled=True),
        lax.all_gather(value_basis, "fs", axis=0, tiled=True),
    )
    lifted_o = jnp.dot(all_heads, whole_o, preferred_element_type=jnp.float32)
    part_o = split_product(lifted_o, out_cot)
    lifted_v = jnp.dot(all_latent, whole_v, preferred_element_type=jnp.float32)
    part_v = split_product(lifted_v, value_cot)
    count_o = rows_out * lax.axis_size("fs") * width_out * lax.axis_size("tp")
    count_v = rows_value * lax.axis_size("fs") * head_cols * lax.axis_size("tp")
    proj_o, proj_v = (
        lax.psum(part_o.astype(jnp.bfloat16), "fs").astype(jnp.float32),
        lax.psum(part_v.astype(jnp.bfloat16), "fs").astype(jnp.float32),
    )
    mean_o, square_o, direction_o = moments(proj_o, out_mean, out_square)
    mean_v, square_v, direction_v = moments(proj_v, value_mean, value_square)
    update_o = jnp.dot(out_basis.astype(jnp.float32), direction_o, precision=lax.Precision.HIGHEST)
    update_v = jnp.dot(
        value_basis.astype(jnp.float32), direction_v, precision=lax.Precision.HIGHEST
    )
    total_o, total_v = lax.psum(
        (jnp.sum(update_o * update_o), jnp.sum(update_v * update_v)), ("fs", "tp")
    )
    step_o = LEARN_RATE * update_o * lax.rsqrt(total_o / count_o + EPS_RMS)
    step_v = LEARN_RATE * update_v * lax.rsqrt(total_v / count_v + EPS_RMS)
    new_o = out_weight - step_o
    new_v = value_up_matrix - step_v
    copy_o, copy_v = (
        lax.all_gather(new_o.astype(jnp.bfloat16), "fs", axis=0, tiled=True),
        lax.all_gather(new_v.astype(jnp.bfloat16), "fs", axis=0, tiled=True),
    )
    return (step_o, new_o, copy_o, mean_o, square_o, step_v, new_v, copy_v, mean_v, square_v)


def solution(mesh):
    placed = (
        P("fs", "tp"),
        P("fs", "tp"),
        P("fs", "tp"),
        P("fs", "tp"),
        P("fs", "tp"),
        P("fs", "tp"),
        P("fs", None),
        P("fs", None),
        P(None, "tp"),
        P(None, "tp"),
        P(None, "tp"),
        P(None, "tp"),
    )
    return jax.shard_map(
        per_device,
        mesh=mesh,
        in_specs=placed,
        out_specs=(
            P("fs", "tp"),
            P("fs", "tp"),
            P(None, "tp"),
            P(None, "tp"),
            P(None, "tp"),
            P("fs", "tp"),
            P("fs", "tp"),
            P(None, "tp"),
            P(None, "tp"),
            P(None, "tp"),
        ),
        check_vma=False,
    )
```

profile of v0, /device:TPU:0, one launch (start us, length us, event | category | flops | bytes accessed | tf_op | source)
XLA Modules:
  0.0 352.1 jit_solution(6366198598271107823)
XLA Ops:
  9.5 17.5 %all_gather.22 = bf16[1024,256]{1,0:T(8,128)(2,1)} all-gather(bf16[128,256]{1,0:T(8,128)(2,1)S(1)} %copy-done.11), channel_id=1, replica_groups=mesh['fs'=8,'tp'=4] {'fs'}, dimensions={0}, use_global_device_ids=true | all-gather | bytes 589824 | tf_op jit(solution)/shard_map/all_gather | solution.py:49
  27.0 29.3 %all-gather.12.cloned.1.call-done = bf16[1536,1024]{1,0:T(8,128)(2,1)} async-done(((bf16[1536,256]{1,0:T(8,128)(2,1)}), bf16[1536,1024]{1,0:T(8,128)(2,1)}) %all-gather.12.cloned.1.call-update) | async-done | bytes 3145744 | tf_op jit(solution)/shard_map/all_gather | solution.py:45
  56.3 3.1 fusion.21
  60.0 1.3 fusion.1
  61.3 18.8 %all-gather.8.cloned.1.call-done = bf16[2048,256]{1,0:T(8,128)(2,1)} async-done(((bf16[256,256]{1,0:T(8,128)(2,1)}), bf16[2048,256]{1,0:T(8,128)(2,1)}) %all-gather.8.cloned.1.call-update) | async-done | bytes 1048592 | tf_op jit(solution)/shard_map/all_gather | solution.py:48
  80.2 71.4 %all-gather.6.cloned.1.call-done = bf16[1536,2048]{1,0:T(8,128)(2,1)} async-done(((bf16[1536,512]{1,0:T(8,128)(2,1)}), bf16[1536,2048]{1,0:T(8,128)(2,1)}) %all-gather.6.cloned.1.call-update) | async-done | bytes 6291472 | tf_op jit(solution)/shard_map/all_gather | solution.py:44
  151.5 4.9 %fusion.20 = f32[1536,256]{1,0:T(8,128)S(1)} fusion(bf16[1536,2048]{1,0:T(8,128)(2,1)} %all-gather.6.cloned.1.call-done, bf16[2048,256]{1,0:T(8,128)(2,1)} %all-gather.8.cloned.1.call-done), kind=kOutput, calls=%fused_computation.32 | convolution fusion | flops 1610612736 | bytes 8912896 | tf_op jit(solution)/shard_map/dot_general | solution.py:51
  156.5 1.0 fusion.16
  157.5 1.8 fusion
  160.2 57.0 %all-reduce.4.cloned.1.call-done = (bf16[256,1024]{1,0:T(8,128)(2,1)}, bf16[256,512]{1,0:T(8,128)(2,1)}) async-done(((bf16[256,1024]{1,0:T(8,128)(2,1)}, bf16[256,512]{1,0:T(8,128)(2,1)}), (bf16[256,1024]{1,0:T(8,128)(2,1)}, bf16[256,512]{1,0:T(8,128)(2,1)})) %all-reduce.4.cloned.1.call-update) | async-done | bytes 786448 | tf_op jit(solution)/shard_map/psum | solution.py:58
  217.3 2.1 fusion.3
  219.4 2.6 multiply_reduce_fusion
  223.0 1.2 multiply_reduce_fusion.1
  224.2 39.5 %all-reduce = (f32[]{:T(128)}, f32[]{:T(128)}) all-reduce(f32[]{:T(128)} %get-tuple-element.34, f32[]{:T(128)} %get-tuple-element.36), channel_id=1, replica_groups=mesh['fs'=8,'tp'=4] {'fs','tp'}, use_global_device_ids=true, to_apply=%region_2.0 | all-reduce | flops 2 | bytes 16 | tf_op jit(solution)/shard_map/psum | solution.py:67
  264.4 1.8 fusion.18
  266.3 2.5 copy.22
  269.5 3.2 fusion.19
  272.8 2.6 copy.24
  275.4 2.6 copy.25
  277.9 1.8 copy.27
  280.6 9.7 %all-gather.14.cloned.1.call-done = bf16[1024,512]{0,1:T(8,128)(2,1)} async-done(((bf16[128,512]{0,1:T(8,128)(2,1)}), bf16[1024,512]{0,1:T(8,128)(2,1)}) %all-gather.14.cloned.1.call-update) | async-done | bytes 1048592 | tf_op jit(solution)/shard_map/all_gather | solution.py:76
  290.3 2.3 copy.29
  292.6 46.4 %all-gather.10.cloned.1.call-done = bf16[2048,1024]{0,1:T(8,128)(2,1)} async-done(((bf16[256,1024]{0,1:T(8,128)(2,1)}), bf16[2048,1024]{0,1:T(8,128)(2,1)}) %all-gather.10.cloned.1.call-update) | async-done | bytes 4194320 | tf_op jit(solution)/shard_map/all_gather | solution.py:75
  338.9 6.4 %copy.26 = bf16[2048,1024]{1,0:T(8,128)(2,1)} copy(bf16[2048,1024]{0,1:T(8,128)(2,1)} %all-gather.10.cloned.1.call-done) | data formatting | bytes 8388608
  (42 shorter events, 5.6 us)
Async XLA Ops:
  7.2 149.3 %copy-start = (bf16[1536,1024]{1,0:T(8,128)(2,1)S(1)}, bf16[1536,1024]{1,0:T(8,128)(2,1)}, u32[]{:S(2)}) copy-start(bf16[1536,1024]{1,0:T(8,128)(2,1)} %param.13) | copy-start | bytes 9437188
  7.2 2.3 copy-start.11
  7.2 49.1 %all-gather.12.cloned.1.call-start = ((), (), s32[]{:S(2)}) async-start(), calls=%async_computation.3 | async-start | bytes 3932160 | tf_op jit(solution)/shard_map/all_gather | solution.py:45
  7.9 72.2 %all-gather.8.cloned.1.call-start = ((), (), s32[]{:S(2)}) async-start(), calls=%async_computation.1 | async-start | bytes 1179648 | tf_op jit(solution)/shard_map/all_gather | solution.py:48
  8.7 142.8 %all-gather.6.cloned.1.call-start = ((), (), s32[]{:S(2)}) async-start(), calls=%async_computation | async-start | bytes 7864320 | tf_op jit(solution)/shard_map/all_gather | solution.py:44
  9.4 207.9 %all-reduce.4.cloned.1.call-start = ((), (), s32[]{:S(2)}) async-start(), calls=%async_computation.5 | async-start | bytes 1572864 | tf_op jit(solution)/shard_map/psum | solution.py:58
  56.3 3.1 copy-start.1
  157.5 1.9 copy-start.12
  159.3 130.9 %all-gather.14.cloned.1.call-start = ((), (), s32[]{:S(2)}) async-start(), calls=%async_computation.4 | async-start | bytes 1179648 | tf_op jit(solution)/shard_map/all_gather | solution.py:76
  217.3 2.1 copy-start.7
  219.3 2.7 copy-start.2
  219.4 2.7 copy-start.3
  219.4 2.6 copy-start.8
  219.4 2.6 copy-start.9
  219.4 2.6 copy-start.10
  222.2 0.8 copy-start.4
  222.2 2.0 copy-start.5
  266.3 72.6 %all-gather.10.cloned.1.call-start = ((), (), s32[]{:S(2)}) async-start(), calls=%async_computation.2 | async-start | bytes 4718592 | tf_op jit(solution)/shard_map/all_gather | solution.py:75
  275.4 4.4 %copy-start.6 = (f32[128,512]{0,1:T(8,128)S(1)}, f32[128,512]{0,1:T(8,128)}, u32[]{:S(2)}) copy-start(f32[128,512]{0,1:T(8,128)} %get-tuple-element.25) | copy-start | bytes 786436
Sparse Core Ops, SparseCore 0:
  9.8 46.4 all-gather.11
  57.9 22.2 all-gather.7
  82.0 69.4 all-gather.5
  159.5 57.7 all-reduce.3
  266.4 23.8 all-gather.13
  292.3 46.5 all-gather.9
where the time goes:
time: 353 us; the launch traced here: 352 us
  waiting for transfers between devices  235 us (67%)
  blocking collectives  57 us (16%)
  local copies, waits for them, and re-layouts  20.6 us (6%)
  matrix products  16.6 us (5%)
  between operations  15.7 us (4%)
  other arithmetic  7.29 us (2%)
    all_gather x1, waiting for transfers between devices, per_device(): lax.all_gather(attn_out, 'tp', axis=1, tiled=True)  71.4 us
    psum x1, waiting for transfers between devices, per_device(): lax.psum(part_o.astype(jnp.bfloat16), 'fs').astype(jnp.float32)  57 us
    all_gather x1, waiting for transfers between devices, per_device(): lax.all_gather(new_o.astype(jnp.bfloat16), 'fs', axis=0, tiled=True)  46.4 us
    psum x1, blocking collectives, per_device(): lax.psum((jnp.sum(update_o * update_o), jnp.sum(update_v * update_v)), ('...  39.5 us
    all_gather x1, waiting for transfers between devices, per_device(): lax.all_gather(latent, 'tp', axis=1, tiled=True)  29.3 us
    unnamed x34, local copies, waits for them, and re-layouts  20.6 us
    all_gather x1, waiting for transfers between devices, per_device(): lax.all_gather(out_basis, 'fs', axis=0, tiled=True)  18.8 us
    all_gather x1, blocking collectives, per_device(): lax.all_gather(value_basis, 'fs', axis=0, tiled=True)  17.5 us
  transfers between devices with their start and end apart: 6, of which 6 were waited for; matrix products, arithmetic and copies ran while one was open for 6% of the time, Pallas kernels for 0%

commit v1 on v0

--- a/solution.py
+++ b/solution.py
@@ -7,6 +7,11 @@
 MEAN_DECAY = 0.8
 BETA_SQUARE = 0.9
 EPS_RMS = 1e-06
+
+
+def add_all(block, axis):
+    parts = lax.all_gather(block, axis)
+    return jnp.sum(parts, axis=0)
 
 
 def moments(proj, mean_in, square_in):
@@ -55,7 +60,7 @@
     count_o = rows_out * lax.axis_size("fs") * width_out * lax.axis_size("tp")
     count_v = rows_value * lax.axis_size("fs") * head_cols * lax.axis_size("tp")
     proj_o, proj_v = (
-        lax.psum(part_o.astype(jnp.bfloat16), "fs").astype(jnp.float32),
+        add_all(part_o.astype(jnp.bfloat16), "fs").astype(jnp.float32),
         lax.psum(part_v.astype(jnp.bfloat16), "fs").astype(jnp.float32),
     )
     mean_o, square_o, direction_o = moments(proj_o, out_mean, out_square)

time: 353 us -> 395 us (1.12)
  waiting for transfers between devices: 235 us -> 272 us
  other arithmetic: 7.29 us -> 12.6 us
    all_gather x0 -> x1, waiting for transfers between devices: none -> 44.3 us  [add_all(): parts = lax.all_gather(block, axis)]
    psum x1, waiting for transfers between devices: 57 us -> 49.5 us  [per_device(): lax.psum(part_v.astype(jnp.bfloat16), 'fs').astype(jnp.float32)]
    reduce_sum x0 -> x1, other arithmetic: none -> 4 us  [add_all(): return jnp.sum(parts, axis=0)]
    unnamed x34 -> x28, local copies, waits for them, and re-layouts: 20.6 us -> 20.8 us
  transfers between devices with their start and end apart: 6 -> 7, of which waited for: 6 -> 7; matrix products, arithmetic and copies ran while one was open for 6% -> 8% of each run, Pallas kernels for 0% -> 0%
where the time goes in v1:
time: 395 us; the launch traced here: 394 us
  waiting for transfers between devices  272 us (69%)
  blocking collectives  56.8 us (14%)
  local copies, waits for them, and re-layouts  20.8 us (5%)
  matrix products  16.5 us (4%)
  between operations  15.7 us (4%)
  other arithmetic  12.6 us (3%)
    all_gather x1, waiting for transfers between devices, per_device(): lax.all_gather(attn_out, 'tp', axis=1, tiled=True)  71.4 us
    psum x1, waiting for transfers between devices, per_device(): lax.psum(part_v.astype(jnp.bfloat16), 'fs').astype(jnp.float32)  49.5 us
    all_gather x1, waiting for transfers between devices, per_device(): lax.all_gather(new_o.astype(jnp.bfloat16), 'fs', axis=0, tiled=True)  46.5 us
    all_gather x1, waiting for transfers between devices, add_all(): parts = lax.all_gather(block, axis)  44.3 us
    psum x1, blocking collectives, per_device(): lax.psum((jnp.sum(update_o * update_o), jnp.sum(update_v * update_v)), ('...  39.2 us
    all_gather x1, waiting for transfers between devices, per_device(): lax.all_gather(latent, 'tp', axis=1, tiled=True)  29.3 us
    unnamed x28, local copies, waits for them, and re-layouts  20.8 us
    all_gather x1, waiting for transfers between devices, per_device(): lax.all_gather(out_basis, 'fs', axis=0, tiled=True)  18.8 us
  transfers between devices with their start and end apart: 7, of which 7 were waited for; matrix products, arithmetic and copies ran while one was open for 8% of the time, Pallas kernels for 0%

profile of v1, /device:TPU:0, one launch (start us, length us, event | category | flops | bytes accessed | tf_op | source)
XLA Modules:
  0.0 394.2 jit_solution(1463028151386565865)
XLA Ops:
  9.5 17.5 %all_gather.30 = bf16[1024,256]{1,0:T(8,128)(2,1)} all-gather(bf16[128,256]{1,0:T(8,128)(2,1)S(1)} %copy-done.8), channel_id=1, replica_groups=mesh['fs'=8,'tp'=4] {'fs'}, dimensions={0}, use_global_device_ids=true | all-gather | bytes 589824 | tf_op jit(solution)/shard_map/all_gather | solution.py:54
  27.0 29.3 %all-gather.14.cloned.1.call-done = bf16[1536,1024]{1,0:T(8,128)(2,1)} async-done(((bf16[1536,256]{1,0:T(8,128)(2,1)}), bf16[1536,1024]{1,0:T(8,128)(2,1)}) %all-gather.14.cloned.1.call-update) | async-done | bytes 3145744 | tf_op jit(solution)/shard_map/all_gather | solution.py:50
  56.3 3.1 fusion.21
  61.4 18.8 %all-gather.10.cloned.1.call-done = bf16[2048,256]{1,0:T(8,128)(2,1)} async-done(((bf16[256,256]{1,0:T(8,128)(2,1)}), bf16[2048,256]{1,0:T(8,128)(2,1)}) %all-gather.10.cloned.1.call-update) | async-done | bytes 1048592 | tf_op jit(solution)/shard_map/all_gather | solution.py:53
  80.2 71.4 %all-gather.8.cloned.1.call-done = bf16[1536,2048]{1,0:T(8,128)(2,1)} async-done(((bf16[1536,512]{1,0:T(8,128)(2,1)}), bf16[1536,2048]{1,0:T(8,128)(2,1)}) %all-gather.8.cloned.1.call-update) | async-done | bytes 6291472 | tf_op jit(solution)/shard_map/all_gather | solution.py:49
  151.5 4.9 %fusion.20 = f32[1536,256]{1,0:T(8,128)S(1)} fusion(bf16[1536,2048]{1,0:T(8,128)(2,1)} %all-gather.8.cloned.1.call-done, bf16[2048,256]{1,0:T(8,128)(2,1)} %all-gather.10.cloned.1.call-done), kind=kOutput, calls=%fused_computation.32 | convolution fusion | flops 1610612736 | bytes 8912896 | tf_op jit(solution)/shard_map/dot_general | solution.py:56
  157.5 1.8 fusion
  160.2 49.5 %all-reduce.3.cloned.1.call-done = bf16[256,512]{1,0:T(8,128)(2,1)} async-done(((bf16[256,512]{1,0:T(8,128)(2,1)}), bf16[256,512]{1,0:T(8,128)(2,1)}) %all-reduce.3.cloned.1.call-update) | async-done | bytes 262160 | tf_op jit(solution)/shard_map/psum | solution.py:64
  209.7 1.5 fusion.8
  213.3 44.3 %all-gather.18.cloned.1.call-done = bf16[2048,1024]{1,0:T(8,128)(2,1)} async-done(((bf16[256,1024]{1,0:T(8,128)(2,1)}), bf16[2048,1024]{1,0:T(8,128)(2,1)}) %all-gather.18.cloned.1.call-update) | async-done | bytes 4194320 | tf_op jit(solution)/shard_map/all_gather | solution.py:13
  257.7 4.0 %reduce_sum.30 = bf16[256,1024]{1,0:T(8,128)(2,1)} reduce(bf16[8,256,1024]{2,1,0:T(8,128)(2,1)} %bitcast.17, bf16[]{:T(256)} %constant.11.clone.1), dimensions={0}, to_apply=%region_0.0 | reduce | flops 1835008 | bytes 4718594 | tf_op jit(solution)/shard_map/reduce_sum | solution.py:14
  261.7 2.1 fusion.3
  263.8 2.6 multiply_reduce_fusion
  266.4 39.2 %all-reduce = (f32[]{:T(128)}, f32[]{:T(128)}) all-reduce(f32[]{:T(128)} %get-tuple-element.32, f32[]{:T(128)} %get-tuple-element.34), channel_id=1, replica_groups=mesh['fs'=8,'tp'=4] {'fs','tp'}, use_global_device_ids=true, to_apply=%region_2.0 | all-reduce | flops 2 | bytes 16 | tf_op jit(solution)/shard_map/psum | solution.py:72
  306.3 1.8 fusion.18
  308.2 2.5 copy.22
  311.4 3.2 fusion.19
  314.7 2.6 copy.24
  317.3 2.6 copy.25
  319.8 1.8 copy.27
  322.5 9.7 %all-gather.16.cloned.1.call-done = bf16[1024,512]{0,1:T(8,128)(2,1)} async-done(((bf16[128,512]{0,1:T(8,128)(2,1)}), bf16[1024,512]{0,1:T(8,128)(2,1)}) %all-gather.16.cloned.1.call-update) | async-done | bytes 1048592 | tf_op jit(solution)/shard_map/all_gather | solution.py:81
  332.1 2.3 copy.29
  334.4 46.5 %all-gather.12.cloned.1.call-done = bf16[2048,1024]{0,1:T(8,128)(2,1)} async-done(((bf16[256,1024]{0,1:T(8,128)(2,1)}), bf16[2048,1024]{0,1:T(8,128)(2,1)}) %all-gather.12.cloned.1.call-update) | async-done | bytes 4194320 | tf_op jit(solution)/shard_map/all_gather | solution.py:80
  380.9 6.4 %copy.26 = bf16[2048,1024]{1,0:T(8,128)(2,1)} copy(bf16[2048,1024]{0,1:T(8,128)(2,1)} %all-gather.12.cloned.1.call-done) | data formatting | bytes 8388608
  (40 shorter events, 9.2 us)
Async XLA Ops:
  7.2 149.3 %copy-start = (bf16[1536,1024]{1,0:T(8,128)(2,1)S(1)}, bf16[1536,1024]{1,0:T(8,128)(2,1)}, u32[]{:S(2)}) copy-start(bf16[1536,1024]{1,0:T(8,128)(2,1)} %param.13) | copy-start | bytes 9437188
  7.2 2.3 copy-start.8
  7.2 49.1 %all-gather.14.cloned.1.call-start = ((), (), s32[]{:S(2)}) async-start(), calls=%async_computation.3 | async-start | bytes 3932160 | tf_op jit(solution)/shard_map/all_gather | solution.py:50
  7.9 72.2 %all-gather.10.cloned.1.call-start = ((), (), s32[]{:S(2)}) async-start(), calls=%async_computation.1 | async-start | bytes 1179648 | tf_op jit(solution)/shard_map/all_gather | solution.py:53
  8.7 142.8 %all-gather.8.cloned.1.call-start = ((), (), s32[]{:S(2)}) async-start(), calls=%async_computation | async-start | bytes 7864320 | tf_op jit(solution)/shard_map/all_gather | solution.py:49
  9.4 200.3 %all-reduce.3.cloned.1.call-start = ((), (), s32[]{:S(2)}) async-start(), calls=%async_computation.4 | async-start | bytes 524288 | tf_op jit(solution)/shard_map/psum | solution.py:64
  56.3 3.1 copy-start.1
  61.4 196.3 %all-gather.18.cloned.1.call-start = ((), (), s32[]{:S(2)}) async-start(), calls=%async_computation.6 | async-start | bytes 4718592 | tf_op jit(solution)/shard_map/all_gather | solution.py:13
  157.5 1.9 copy-start.9
  159.3 172.8 %all-gather.16.cloned.1.call-start = ((), (), s32[]{:S(2)}) async-start(), calls=%async_computation.5 | async-start | bytes 1179648 | tf_op jit(solution)/shard_map/all_gather | solution.py:81
  211.2 0.8 copy-start.4
  211.2 1.0 copy-start.5
  261.7 2.1 copy-start.7
  263.8 2.6 copy-start.2
  263.8 2.6 copy-start.3
  308.2 72.8 %all-gather.12.cloned.1.call-start = ((), (), s32[]{:S(2)}) async-start(), calls=%async_computation.2 | async-start | bytes 4718592 | tf_op jit(solution)/shard_map/all_gather | solution.py:80
  317.3 4.4 %copy-start.6 = (f32[128,512]{0,1:T(8,128)S(1)}, f32[128,512]{0,1:T(8,128)}, u32[]{:S(2)}) copy-start(f32[128,512]{0,1:T(8,128)} %get-tuple-element.23) | copy-start | bytes 786436
Sparse Core Ops, SparseCore 0:
  9.8 46.4 all-gather.13
  57.9 22.2 all-gather.9
  82.0 69.4 all-gather.7
  154.3 55.4 all-reduce.2
  211.7 45.9 all-gather.17
  308.3 23.8 all-gather.15
  334.3 46.5 all-gather.11
